TPU v7x, 32 devices: a whole 2x2x4 slice. The times are simulated.
32 devices in a mesh: sp: 8 (over z, x), tp: 4 (over y, core).
Axes of the slice: x: 2, y: 2, z: 4, core: 2. Of those that a mesh axis runs over, the one named last changes fastest.
Arguments:
- tokens: bfloat16 [2048, 1024], P(('sp', 'tp')), may hold values from -6 to 6
- norm_gain: float32 [1024], replicated, may hold values from 0.1 to 1.9
- w_query: bfloat16 [1024, 1024], P('sp', 'tp'), may hold values from -0.1875 to 0.1875
- w_key: bfloat16 [1024, 1024], P('sp', 'tp'), may hold values from -0.1875 to 0.1875
- w_value: bfloat16 [1024, 1024], P('sp', 'tp'), may hold values from -0.1875 to 0.1875
- w_forget: bfloat16 [1024, 16], P('sp', 'tp'), may hold values from -0.375 to 0.375
- forget_offset: float32 [16], P('tp'), may hold values from 1 to 3.5
- w_out_t: bfloat16 [1024, 1024], P('sp', 'tp'), may hold values from -0.1875 to 0.1875
- out_gain: float32 [1024], replicated, may hold values from 0.1 to 1.9
Outputs:
- mixed: bfloat16 [2048, 1024], P(('sp', 'tp'))
All inputs are finite; a program needn't handle non-finite values.
Results may differ from a plain program's by a relative error of at most 0.015.
Values may be sent and summed in bfloat16 or wider, within the bound.
A program may use at most 192 MiB of HBM per device.

v0:
```python
import jax
import jax.numpy as jnp
from jax import lax
from jax.sharding import PartitionSpec as P

HEAD_DIM = 64
norm_eps = 1e-06
masked_score = -1e30


def on_whole(shard, axis, dim, work):
    return work(lax.all_gather(shard, axis, axis=dim, tiled=True), jnp.int32(0))


def over_all(section, axis, dim, turn, start):

    def gathered(part):
        return lax.all_gather(part, axis, axis=dim, tiled=True)

    return turn(start, jax.tree.map(gathered, section), jnp.int32(0))


def own_rows(portion, width, axis):
    count = width * lax.axis_size(axis)
    sent = portion(jnp.int32(0), count).astype(jnp.bfloat16)
    return lax.psum_scatter(sent, axis, scatter_dimension=0, tiled=True).astype(jnp.float32)


def rms_norm(values_in, gain_row):
    floats = values_in.astype(jnp.float32)
    scale_row = lax.rsqrt(jnp.mean(floats * floats, axis=-1, keepdims=True) + norm_eps)
    return (floats * scale_row * gain_row).astype(jnp.bfloat16)


def on_device(
    tokens, norm_gain, w_query, w_key, w_value, w_forget, forget_offset, w_out_t, out_gain
):
    normed = rms_norm(tokens, norm_gain)
    width_local = w_query.shape[1]
    heads_local = w_forget.shape[1]
    tok_block = normed.shape[0] * lax.axis_size("tp")
    total_tokens = tok_block * lax.axis_size("sp")
    full_query, full_key, full_value, full_forget, out_weight = (
        lax.all_gather(w_query, "sp", axis=0, tiled=True),
        lax.all_gather(w_key, "sp", axis=0, tiled=True),
        lax.all_gather(w_value, "sp", axis=0, tiled=True),
        lax.all_gather(w_forget, "sp", axis=0, tiled=True),
        lax.all_gather(w_out_t, "sp", axis=0, tiled=True),
    )
    joined = jnp.concatenate([full_query, full_key, full_value, full_forget], axis=1)

    def project(row_piece, first_row):
        return jnp.dot(row_piece, joined, preferred_element_type=jnp.float32)

    projected_cols = on_whole(normed, "tp", 0, project)
    head_shape = (tok_block, heads_local, HEAD_DIM)
    queries = projected_cols[:, :width_local].astype(jnp.bfloat16).reshape(head_shape)
    keys_here = (
        projected_cols[:, width_local : 2 * width_local].astype(jnp.bfloat16).reshape(head_shape)
    )
    values_here = (
        projected_cols[:, 2 * width_local : 3 * width_local]
        .astype(jnp.bfloat16)
        .reshape(head_shape)
    )
    logits = (
        projected_cols[:, 3 * width_local :] + forget_offset + jnp.log(jnp.float32(total_tokens))
    )
    log_gates = jax.nn.log_sigmoid(logits)
    all_gates = lax.all_gather(log_gates, "sp", axis=0, tiled=True)
    cumulative = jnp.cumsum(all_gates, axis=0)
    offset = lax.axis_index("sp") * tok_block
    cum_query = lax.dynamic_slice_in_dim(cumulative, offset, tok_block, 0)
    query_pos = offset + jnp.arange(tok_block, dtype=jnp.int32)
    score_scale = HEAD_DIM ** (-0.5)

    def absorb(state_now, pieces, first_row):
        run_max, run_sum, run_acc = state_now
        key_piece, value_piece = pieces
        span_len = key_piece.shape[0]
        cum_key = lax.dynamic_slice_in_dim(cumulative, first_row, span_len, 0)
        scores = (
            jnp.einsum("qhd,khd->hqk", queries, key_piece, preferred_element_type=jnp.float32)
            * score_scale
        )
        scores = scores + cum_query.T[:, :, None] - cum_key.T[:, None, :]
        key_pos = first_row + jnp.arange(span_len, dtype=jnp.int32)
        allowed = (key_pos[None, :] <= query_pos[:, None])[None]
        scores = jnp.where(allowed, scores, masked_score)
        new_max = jnp.maximum(run_max, jnp.max(scores, axis=-1))
        shares = jnp.where(allowed, jnp.exp(scores - new_max[..., None]), 0.0)
        rescale = jnp.exp(run_max - new_max)
        new_sum = run_sum * rescale + jnp.sum(shares, axis=-1)
        new_acc = run_acc * rescale[..., None] + jnp.einsum(
            "hqk,khd->hqd", shares, value_piece.astype(jnp.float32), precision=lax.Precision.HIGHEST
        )
        return (new_max, new_sum, new_acc)

    start_state = (
        jnp.full((heads_local, tok_block), masked_score, jnp.float32),
        jnp.zeros((heads_local, tok_block), jnp.float32),
        jnp.zeros((heads_local, tok_block, HEAD_DIM), jnp.float32),
    )
    run_max, run_sum, run_acc = over_all((keys_here, values_here), "sp", 0, absorb, start_state)
    attended = (
        (run_acc / run_sum[..., None])
        .transpose(1, 0, 2)
        .reshape(tok_block, width_local)
        .astype(jnp.bfloat16)
    )
    rows_mine = tokens.shape[0]

    def out_term(first_row, row_count):
        block_rows = lax.dynamic_slice_in_dim(attended, first_row, row_count, 0)
        return lax.dot_general(
            block_rows, out_weight, (((1,), (1,)), ((), ())), preferred_element_type=jnp.float32
        )

    projected = own_rows(out_term, rows_mine, "tp")
    return rms_norm(projected, out_gain)


def solution(mesh):
    return jax.shard_map(
        on_device,
        mesh=mesh,
        in_specs=(
            P(("sp", "tp"), None),
            P(),
            P("sp", "tp"),
            P("sp", "tp"),
            P("sp", "tp"),
            P("sp", "tp"),
            P("tp"),
            P("sp", "tp"),
            P(),
        ),
        out_specs=P(("sp", "tp"), None),
        check_vma=False,
    )
```

profile of v0, /device:TPU:0, one launch (start us, length us, event | category | flops | bytes accessed | tf_op | source)
XLA Modules:
  0.0 256.3 jit_solution(14113764363407624056)
XLA Ops:
  6.5 0.0 copy-start.3
  6.5 0.0 copy-start.1
  6.5 0.0 all-gather.3.cloned.1.call-start
  6.5 1.1 fusion.22
  7.6 1.0 fusion.24
  8.6 8.7 %all_gather.27 = bf16[256,1024]{1,0:T(8,128)(2,1)S(1)} all-gather(bf16[64,1024]{1,0:T(8,128)(2,1)S(1)} %fusion.24), channel_id=1, replica_groups=mesh['sp'=8,'tp'=4] {'tp'}, dimensions={0}, use_global_device_ids=true | all-gather | bytes 655360 | tf_op jit(solution)/shard_map/all_gather | solution.py:12
  17.3 32.1 %all_gather.28 = bf16[1024,256]{1,0:T(8,128)(2,1)S(1)} all-gather(bf16[128,256]{1,0:T(8,128)(2,1)} %param.11), channel_id=1, replica_groups=mesh['sp'=8,'tp'=4] {'sp'}, dimensions={0}, use_global_device_ids=true | all-gather | bytes 589824 | tf_op jit(solution)/shard_map/all_gather | solution.py:44
  49.4 31.6 %all_gather.29 = bf16[1024,256]{1,0:T(8,128)(2,1)S(1)} all-gather(bf16[128,256]{1,0:T(8,128)(2,1)} %param.12), channel_id=1, replica_groups=mesh['sp'=8,'tp'=4] {'sp'}, dimensions={0}, use_global_device_ids=true | all-gather | bytes 589824 | tf_op jit(solution)/shard_map/all_gather | solution.py:45
  81.0 31.4 %all_gather.30 = bf16[1024,256]{1,0:T(8,128)(2,1)S(1)} all-gather(bf16[128,256]{1,0:T(8,128)(2,1)} %param.13), channel_id=1, replica_groups=mesh['sp'=8,'tp'=4] {'sp'}, dimensions={0}, use_global_device_ids=true | all-gather | bytes 589824 | tf_op jit(solution)/shard_map/all_gather | solution.py:46
  112.4 21.0 %all_gather.31 = bf16[1024,4]{0,1:T(4,128)(2,1)S(1)} all-gather(bf16[128,4]{0,1:T(4,128)(2,1)} %param.14), channel_id=1, replica_groups=mesh['sp'=8,'tp'=4] {'sp'}, dimensions={0}, use_global_device_ids=true | all-gather | bytes 9216 | tf_op jit(solution)/shard_map/all_gather | solution.py:47
  133.4 0.2 copy.11
  133.6 0.8 fusion.36
  134.4 0.7 fusion.35
  135.1 0.0 all-gather.3.cloned.1.call-update
  135.2 0.0 all-gather.5.cloned.1.call-start
  135.2 0.7 all-gather.5.cloned.1.call-update
  135.9 0.0 reduce-scatter.2.cloned.1.call-start
  136.0 0.0 copy-done.3
  136.0 0.1 fusion.28
  136.1 30.9 %all_gather.33 = f32[2048,4]{0,1:T(4,128)S(1)} all-gather(f32[256,4]{0,1:T(4,128)S(1)} %fusion.28), channel_id=1, replica_groups=mesh['sp'=8,'tp'=4] {'sp'}, dimensions={0}, use_global_device_ids=true | all-gather | bytes 36864 | tf_op jit(solution)/shard_map/all_gather | solution.py:70
  167.0 1.1 reduce-window.6
  168.1 0.2 slice_reduce_fusion
  168.3 0.2 reduce-window.9
  168.5 0.1 add_bitcast_fusion
  168.6 0.4 iota_compare_fusion
  168.9 0.0 copy-done.1
  168.9 31.6 %all_gather.35 = bf16[1024,256]{1,0:T(8,128)(2,1)S(1)} all-gather(bf16[128,256]{1,0:T(8,128)(2,1)S(1)} %copy-done.1), channel_id=1, replica_groups=mesh['sp'=8,'tp'=4] {'sp'}, dimensions={0}, use_global_device_ids=true | all-gather | bytes 589824 | tf_op jit(solution)/shard_map/all_gather | solution.py:48
  200.5 0.0 all-gather.3.cloned.1.call-done
  200.5 3.9 %fusion.2 = (f32[4,256]{1,0:T(4,128)S(1)}, f32[4,256,2048]{2,1,0:T(8,128)S(1)}) fusion(f32[4,2048]{1,0:T(4,128)S(1)} %bitcast.38, f32[4,256]{1,0:T(4,128)S(1)} %constant_dynamic-slice_fusion, pred[256,2048]{1,0:T(8,128)(4,1)S(1)} %iota_compare_fusion, bf16[256,4,64]{0,2,1:T(8,128)(2,1)S(1)} %bitcast.44, bf16[2048,4,64]{0,2,1:T(8,128)(2,1)} %all-gather.3.cloned.1.call-done), kind=kOutput, calls=%fused_computation.4 | convolution fusion | flops 278920192 | bytes 10133504 | tf_op jit(solution)/shard_map/qhd,khd->hqk/dot_general | solution.py:83
  204.4 0.0 copy-start
  204.4 3.2 %copy-done = f32[4,256,2048]{2,1,0:T(8,128)} copy-done((f32[4,256,2048]{2,1,0:T(8,128)}, f32[4,256,2048]{2,1,0:T(8,128)S(1)}, u32[]{:S(2)}) %copy-start) | copy-done | bytes 8388632
  207.6 3.2 %fusion = f32[4,256]{1,0:T(4,128)S(1)} fusion(f32[4,256,2048]{2,1,0:T(8,128)S(1)} %get-tuple-element.13, f32[4,256]{1,0:T(4,128)S(1)} %get-tuple-element.9, f32[4,2048]{1,0:T(4,128)S(1)} %bitcast.39, f32[4,256]{1,0:T(4,128)S(1)} %constant_dynamic-slice_fusion, pred[256,2048]{1,0:T(8,128)(4,1)S(1)} %iota_compare_fusion), kind=kLoop, calls=%fused_computation.2 | loop fusion | flops 14679040 | bytes 8957952 | tf_op jit(solution)/shard_map/reduce_sum | solution.py:93
  210.8 3.8 %all-gather.5.cloned.1.call-done = bf16[2048,4,64]{0,2,1:T(8,128)(2,1)} async-done(((bf16[256,4,64]{0,2,1:T(8,128)(2,1)}), bf16[2048,4,64]{0,2,1:T(8,128)(2,1)}) %all-gather.5.cloned.1.call-update) | async-done | bytes 1048592 | tf_op jit(solution)/shard_map/all_gather | solution.py:18
  214.7 0.0 copy-start.2
  214.7 10.4 %fusion.21 = bf16[256,4,64]{0,2,1:T(8,128)(2,1)S(1)} fusion(bf16[2048,4,64]{0,2,1:T(8,128)(2,1)} %all-gather.5.cloned.1.call-done, f32[4,256,2048]{2,1,0:T(8,128)} %copy-done, f32[4,256]{1,0:T(4,128)S(1)} %get-tuple-element.9, f32[4,2048]{1,0:T(4,128)S(1)} %bitcast.40, f32[4,256]{1,0:T(4,128)S(1)} %constant_dynamic-slice_fusion, ...), kind=kOutput, calls=%fused_computation.25 | convolution fusion | flops 1623392256 | bytes 10141696 | tf_op jit(solution)/shard_map/hqk,khd->hqd/dot_general | solution.py:94
  225.1 1.2 convolution_convert_fusion
  226.2 0.0 reduce-scatter.2.cloned.1.call-update
  226.2 20.9 %reduce-scatter.2.cloned.1.call-done = bf16[64,1024]{1,0:T(8,128)(2,1)} async-done(((bf16[256,1024]{1,0:T(8,128)(2,1)}), bf16[64,1024]{1,0:T(8,128)(2,1)}) %reduce-scatter.2.cloned.1.call-update) | async-done | bytes 131088 | tf_op jit(solution)/shard_map/reduce_scatter | solution.py:26
  247.1 1.0 fusion.25
  248.1 0.0 copy-done.2
  248.2 1.7 fusion.27
  (8 shorter events, 0.1 us)
Async XLA Ops:
  6.5 129.5 %copy-start.3 = (f32[4]{0:T(128)S(1)}, f32[4]{0:T(128)}, u32[]{:S(2)}) copy-start(f32[4]{0:T(128)} %param.15) | copy-start | bytes 52
  6.5 162.4 %copy-start.1 = (bf16[128,256]{1,0:T(8,128)(2,1)S(1)}, bf16[128,256]{1,0:T(8,128)(2,1)}, u32[]{:S(2)}) copy-start(bf16[128,256]{1,0:T(8,128)(2,1)} %param.16) | copy-start | bytes 196612
  6.5 194.0 %all-gather.3.cloned.1.call-start = ((), (), s32[]{:S(2)}) async-start(), calls=%async_computation.1 | async-start | bytes 1179648 | tf_op jit(solution)/shard_map/all_gather | solution.py:18
  135.2 79.5 %all-gather.5.cloned.1.call-start = ((), (), s32[]{:S(2)}) async-start(), calls=%async_computation.2 | async-start | bytes 1179648 | tf_op jit(solution)/shard_map/all_gather | solution.py:18
  135.9 111.2 %reduce-scatter.2.cloned.1.call-start = ((), (), s32[]{:S(2)}) async-start(), calls=%async_computation.3 | async-start | bytes 655360 | tf_op jit(solution)/shard_map/reduce_scatter | solution.py:26
  204.4 3.2 %copy-start = (f32[4,256,2048]{2,1,0:T(8,128)}, f32[4,256,2048]{2,1,0:T(8,128)S(1)}, u32[]{:S(2)}) copy-start(f32[4,256,2048]{2,1,0:T(8,128)S(1)} %get-tuple-element.13) | copy-start | bytes 25165828
  214.7 33.5 %copy-start.2 = (f32[1024]{0:T(1024)S(1)}, f32[1024]{0:T(1024)}, u32[]{:S(2)}) copy-start(f32[1024]{0:T(1024)} %param.17) | copy-start | bytes 12292
Sparse Core Ops, SparseCore 0:
  135.3 37.4 all-gather.2
  174.8 39.7 all-gather.4
  226.4 20.6 reduce-scatter.1
where the time goes:
time: 257 us; the launch traced here: 256 us
  blocking collectives  187 us (73%)
  waiting for transfers between devices  25.4 us (10%)
  matrix products  16.2 us (6%)
  between operations  13.2 us (5%)
  other arithmetic  9.86 us (4%)
  local copies, waits for them, and re-layouts  4.32 us (2%)
    all_gather x1, blocking collectives, on_device(): lax.all_gather(w_query, 'sp', axis=0, tiled=True)  32.1 us
    all_gather x1, blocking collectives, on_device(): lax.all_gather(w_key, 'sp', axis=0, tiled=True)  31.6 us
    all_gather x1, blocking collectives, on_device(): lax.all_gather(w_out_t, 'sp', axis=0, tiled=True)  31.6 us
    all_gather x1, blocking collectives, on_device(): lax.all_gather(w_value, 'sp', axis=0, tiled=True)  31.4 us
    all_gather x1, blocking collectives, on_device(): all_gates = lax.all_gather(log_gates, 'sp', axis=0, tiled=True)  30.9 us
    all_gather x1, blocking collectives, on_device(): lax.all_gather(w_forget, 'sp', axis=0, tiled=True)  21 us
    reduce_scatter x1, waiting for transfers between devices, own_rows(): lax.psum_scatter(sent, axis, scatter_dimension=0, tiled=True)  20.9 us
    dot_general x1, matrix products, absorb(): jnp.einsum('hqk,khd->hqd', shares, value_piece.astype(jnp.float32), preci...  10.4 us
  transfers between devices with their start and end apart: 3, of which 2 were waited for; matrix products, arithmetic and copies ran while one was open for 4% of the time, Pallas kernels for 0%

commit v1 on v0

--- a/solution.py
+++ b/solution.py
@@ -6,6 +6,16 @@
 HEAD_DIM = 64
 norm_eps = 1e-06
 masked_score = -1e30
+
+
+def gather_by_hops(x, mesh_axis, along):
+    devices = lax.axis_size(mesh_axis)
+    block, tiles = (x, [x])
+    for _ in range(devices - 1):
+        block = lax.ppermute(block, mesh_axis, [(i, (i + 1) % devices) for i in range(devices)])
+        tiles.insert(0, block)
+    merged = jnp.concatenate(tiles, axis=along)
+    return jnp.roll(merged, (lax.axis_index(mesh_axis) + 1) * x.shape[along], axis=along)
 
 
 def on_whole(shard, axis, dim, work):
@@ -67,7 +77,7 @@
         projected_cols[:, 3 * width_local :] + forget_offset + jnp.log(jnp.float32(total_tokens))
     )
     log_gates = jax.nn.log_sigmoid(logits)
-    all_gates = lax.all_gather(log_gates, "sp", axis=0, tiled=True)
+    all_gates = gather_by_hops(log_gates, "sp", 0)
     cumulative = jnp.cumsum(all_gates, axis=0)
     offset = lax.axis_index("sp") * tok_block
     cum_query = lax.dynamic_slice_in_dim(cumulative, offset, tok_block, 0)

time: 257 us -> 262 us (1.019)
  waiting for transfers between devices: 25.4 us -> 60.5 us
  blocking collectives: 187 us -> 157 us
    ppermute x0 -> x7, waiting for transfers between devices: none -> 37.7 us  [gather_by_hops(): lax.ppermute(block, mesh_axis, [(i, (i + 1) % devices) for i in range(dev...]
    all_gather x1 -> x0, blocking collectives: 30.9 us -> none  [on_device(): all_gates = lax.all_gather(log_gates, 'sp', axis=0, tiled=True)]
    all_gather x2, waiting for transfers between devices: 3.82 us -> 0.04 us  [gathered(): return lax.all_gather(part, axis, axis=dim, tiled=True)]
  transfers between devices with their start and end apart: 3 -> 10, of which waited for: 2 -> 7; matrix products, arithmetic and copies ran while one was open for 4% -> 4% of each run, Pallas kernels for 0% -> 0%
where the time goes in v1:
time: 262 us; the launch traced here: 261 us
  blocking collectives  157 us (60%)
  waiting for transfers between devices  60.5 us (23%)
  matrix products  16.2 us (6%)
  between operations  13.3 us (5%)
  other arithmetic  10.1 us (4%)
  local copies, waits for them, and re-layouts  4.46 us (2%)
    ppermute x7, waiting for transfers between devices, gather_by_hops(): lax.ppermute(block, mesh_axis, [(i, (i + 1) % devices) for i in range(dev...  37.7 us
    all_gather x1, blocking collectives, on_device(): lax.all_gather(w_query, 'sp', axis=0, tiled=True)  32.1 us
    all_gather x1, blocking collectives, on_device(): lax.all_gather(w_out_t, 'sp', axis=0, tiled=True)  31.8 us
    all_gather x1, blocking collectives, on_device(): lax.all_gather(w_key, 'sp', axis=0, tiled=True)  31.6 us
    all_gather x1, blocking collectives, on_device(): lax.all_gather(w_value, 'sp', axis=0, tiled=True)  31.4 us
    reduce_scatter x1, waiting for transfers between devices, own_rows(): lax.psum_scatter(sent, axis, scatter_dimension=0, tiled=True)  22.8 us
    all_gather x1, blocking collectives, on_device(): lax.all_gather(w_forget, 'sp', axis=0, tiled=True)  21 us
    dot_general x1, matrix products, absorb(): jnp.einsum('hqk,khd->hqd', shares, value_piece.astype(jnp.float32), preci...  10.4 us
  transfers between devices with their start and end apart: 10, of which 7 were waited for; matrix products, arithmetic and copies ran while one was open for 4% of the time, Pallas kernels for 0%

profile of v1, /device:TPU:0, one launch (start us, length us, event | category | flops | bytes accessed | tf_op | source)
XLA Modules:
  0.0 261.3 jit_solution(3001031216255157700)
XLA Ops:
  6.5 0.0 copy-start.2
  6.5 0.0 copy-start.1
  6.5 0.0 all-gather.3.cloned.1.call-start
  6.5 1.1 fusion.22
  7.6 1.0 fusion.24
  8.6 8.7 %all_gather.24 = bf16[256,1024]{1,0:T(8,128)(2,1)S(1)} all-gather(bf16[64,1024]{1,0:T(8,128)(2,1)S(1)} %fusion.24), channel_id=1, replica_groups=mesh['sp'=8,'tp'=4] {'tp'}, dimensions={0}, use_global_device_ids=true | all-gather | bytes 655360 | tf_op jit(solution)/shard_map/all_gather | solution.py:22
  17.3 32.1 %all_gather.25 = bf16[1024,256]{1,0:T(8,128)(2,1)S(1)} all-gather(bf16[128,256]{1,0:T(8,128)(2,1)} %param.11), channel_id=1, replica_groups=mesh['sp'=8,'tp'=4] {'sp'}, dimensions={0}, use_global_device_ids=true | all-gather | bytes 589824 | tf_op jit(solution)/shard_map/all_gather | solution.py:54
  49.4 31.6 %all_gather.26 = bf16[1024,256]{1,0:T(8,128)(2,1)S(1)} all-gather(bf16[128,256]{1,0:T(8,128)(2,1)} %param.12), channel_id=1, replica_groups=mesh['sp'=8,'tp'=4] {'sp'}, dimensions={0}, use_global_device_ids=true | all-gather | bytes 589824 | tf_op jit(solution)/shard_map/all_gather | solution.py:55
  81.0 31.4 %all_gather.27 = bf16[1024,256]{1,0:T(8,128)(2,1)S(1)} all-gather(bf16[128,256]{1,0:T(8,128)(2,1)} %param.13), channel_id=1, replica_groups=mesh['sp'=8,'tp'=4] {'sp'}, dimensions={0}, use_global_device_ids=true | all-gather | bytes 589824 | tf_op jit(solution)/shard_map/all_gather | solution.py:56
  112.4 21.0 %all_gather.28 = bf16[1024,4]{0,1:T(4,128)(2,1)S(1)} all-gather(bf16[128,4]{0,1:T(4,128)(2,1)} %param.14), channel_id=1, replica_groups=mesh['sp'=8,'tp'=4] {'sp'}, dimensions={0}, use_global_device_ids=true | all-gather | bytes 9216 | tf_op jit(solution)/shard_map/all_gather | solution.py:57
  133.4 0.2 copy.11
  133.6 0.8 fusion.36
  134.4 0.7 fusion.35
  135.1 0.0 all-gather.3.cloned.1.call-update
  135.2 0.0 all-gather.5.cloned.1.call-start
  135.2 0.0 copy-done.2
  135.2 0.1 fusion.28
  135.3 0.1 collective-permute-start
  135.4 6.3 %collective-permute-done = f32[256,4]{0,1:T(4,128)S(1)} collective-permute-done((f32[256,4]{0,1:T(4,128)S(1)}, f32[256,4]{0,1:T(4,128)S(1)}, u32[]{:S(2)}, u32[]{:S(2)}) %collective-permute-start) | collective-permute-done | bytes 4128 | tf_op jit(solution)/shard_map/ppermute | solution.py:15
  141.7 0.0 collective-permute-start.1
  141.7 6.3 %collective-permute-done.1 = f32[256,4]{0,1:T(4,128)S(1)} collective-permute-done((f32[256,4]{0,1:T(4,128)S(1)}, f32[256,4]{0,1:T(4,128)S(1)}, u32[]{:S(2)}, u32[]{:S(2)}) %collective-permute-start.1) | collective-permute-done | bytes 4128 | tf_op jit(solution)/shard_map/ppermute | solution.py:15
  148.0 0.0 collective-permute-start.2
  148.0 6.3 %collective-permute-done.2 = f32[256,4]{0,1:T(4,128)S(1)} collective-permute-done((f32[256,4]{0,1:T(4,128)S(1)}, f32[256,4]{0,1:T(4,128)S(1)}, u32[]{:S(2)}, u32[]{:S(2)}) %collective-permute-start.2) | collective-permute-done | bytes 4128 | tf_op jit(solution)/shard_map/ppermute | solution.py:15
  154.3 0.0 collective-permute-start.3
  154.3 0.0 all-gather.5.cloned.1.call-update
  154.3 0.0 reduce-scatter.2.cloned.1.call-start
  154.4 6.3 %collective-permute-done.3 = f32[256,4]{0,1:T(4,128)S(1)} collective-permute-done((f32[256,4]{0,1:T(4,128)S(1)}, f32[256,4]{0,1:T(4,128)S(1)}, u32[]{:S(2)}, u32[]{:S(2)}) %collective-permute-start.3) | collective-permute-done | bytes 4128 | tf_op jit(solution)/shard_map/ppermute | solution.py:15
  160.7 0.0 collective-permute-start.4
  160.7 6.4 %collective-permute-done.4 = f32[256,4]{0,1:T(4,128)S(1)} collective-permute-done((f32[256,4]{0,1:T(4,128)S(1)}, f32[256,4]{0,1:T(4,128)S(1)}, u32[]{:S(2)}, u32[]{:S(2)}) %collective-permute-start.4) | collective-permute-done | bytes 4128 | tf_op jit(solution)/shard_map/ppermute | solution.py:15
  167.1 0.0 collective-permute-start.5
  167.1 0.4 iota_compare_fusion
  167.5 6.0 %collective-permute-done.5 = f32[256,4]{0,1:T(4,128)S(1)} collective-permute-done((f32[256,4]{0,1:T(4,128)S(1)}, f32[256,4]{0,1:T(4,128)S(1)}, u32[]{:S(2)}, u32[]{:S(2)}) %collective-permute-start.5) | collective-permute-done | bytes 4128 | tf_op jit(solution)/shard_map/ppermute | solution.py:15
  173.5 0.0 collective-permute-start.6
  173.5 0.0 copy-done.1
  173.5 31.8 %all_gather.31 = bf16[1024,256]{1,0:T(8,128)(2,1)S(1)} all-gather(bf16[128,256]{1,0:T(8,128)(2,1)S(1)} %copy-done.1), channel_id=1, replica_groups=mesh['sp'=8,'tp'=4] {'sp'}, dimensions={0}, use_global_device_ids=true | all-gather | bytes 589824 | tf_op jit(solution)/shard_map/all_gather | solution.py:58
  205.3 0.0 collective-permute-done.6
  205.4 0.1 constant_dynamic-update-slice_fusion.8
  205.6 0.1 constant_dynamic-update-slice_fusion
  205.7 1.2 reduce-window.6
  206.9 0.2 slice_reduce_fusion
  207.0 0.2 reduce-window.9
  207.2 0.1 add_bitcast_fusion
  207.4 0.0 all-gather.3.cloned.1.call-done
  207.4 3.8 %fusion.2 = (f32[4,256]{1,0:T(4,128)S(1)}, f32[4,256,2048]{2,1,0:T(8,128)S(1)}) fusion(f32[4,2048]{1,0:T(4,128)S(1)} %bitcast.39, f32[4,256]{1,0:T(4,128)S(1)} %constant_dynamic-slice_fusion, pred[256,2048]{1,0:T(8,128)(4,1)S(1)} %iota_compare_fusion, bf16[256,4,64]{0,2,1:T(8,128)(2,1)S(1)} %bitcast.44, bf16[2048,4,64]{0,2,1:T(8,128)(2,1)} %all-gather.3.cloned.1.call-done), kind=kOutput, calls=%fused_computation.4 | convolution fusion | flops 278920192 | bytes 10133504 | tf_op jit(solution)/shard_map/qhd,khd->hqk/dot_general | solution.py:93
  211.2 0.0 copy-start
  211.3 3.2 %copy-done = f32[4,256,2048]{2,1,0:T(8,128)} copy-done((f32[4,256,2048]{2,1,0:T(8,128)}, f32[4,256,2048]{2,1,0:T(8,128)S(1)}, u32[]{:S(2)}) %copy-start) | copy-done | bytes 8388632
  214.5 3.2 %fusion = f32[4,256]{1,0:T(4,128)S(1)} fusion(f32[4,256,2048]{2,1,0:T(8,128)S(1)} %get-tuple-element.13, f32[4,256]{1,0:T(4,128)S(1)} %get-tuple-element.9, f32[4,2048]{1,0:T(4,128)S(1)} %bitcast.40, f32[4,256]{1,0:T(4,128)S(1)} %constant_dynamic-slice_fusion, pred[256,2048]{1,0:T(8,128)(4,1)S(1)} %iota_compare_fusion), kind=kLoop, calls=%fused_computation.2 | loop fusion | flops 14679040 | bytes 8957952 | tf_op jit(solution)/shard_map/reduce_sum | solution.py:103
  217.7 0.0 all-gather.5.cloned.1.call-done
  217.7 0.0 copy-start.3
  217.7 10.4 %fusion.21 = bf16[256,4,64]{0,2,1:T(8,128)(2,1)S(1)} fusion(bf16[2048,4,64]{0,2,1:T(8,128)(2,1)} %all-gather.5.cloned.1.call-done, f32[4,256,2048]{2,1,0:T(8,128)} %copy-done, f32[4,256]{1,0:T(4,128)S(1)} %get-tuple-element.9, f32[4,2048]{1,0:T(4,128)S(1)} %bitcast.41, f32[4,256]{1,0:T(4,128)S(1)} %constant_dynamic-slice_fusion, ...), kind=kOutput, calls=%fused_computation.25 | convolution fusion | flops 1623392256 | bytes 10141696 | tf_op jit(solution)/shard_map/hqk,khd->hqd/dot_general | solution.py:104
  228.1 1.1 convolution_convert_fusion
  229.3 0.0 reduce-scatter.2.cloned.1.call-update
  229.3 22.8 %reduce-scatter.2.cloned.1.call-done = bf16[64,1024]{1,0:T(8,128)(2,1)} async-done(((bf16[256,1024]{1,0:T(8,128)(2,1)}), bf16[64,1024]{1,0:T(8,128)(2,1)}) %reduce-scatter.2.cloned.1.call-update) | async-done | bytes 131088 | tf_op jit(solution)/shard_map/reduce_scatter | solution.py:36
  252.0 1.0 fusion.25
  253.1 0.0 copy-done.3
  253.1 1.7 fusion.27
  (23 shorter events, 0.2 us)
Async XLA Ops:
  6.5 128.7 %copy-start.2 = (f32[4]{0:T(128)S(1)}, f32[4]{0:T(128)}, u32[]{:S(2)}) copy-start(f32[4]{0:T(128)} %param.15) | copy-start | bytes 52
  6.5 167.0 %copy-start.1 = (bf16[128,256]{1,0:T(8,128)(2,1)S(1)}, bf16[128,256]{1,0:T(8,128)(2,1)}, u32[]{:S(2)}) copy-start(bf16[128,256]{1,0:T(8,128)(2,1)} %param.16) | copy-start | bytes 196612
  6.5 200.8 %all-gather.3.cloned.1.call-start = ((), (), s32[]{:S(2)}) async-start(), calls=%async_computation.1 | async-start | bytes 1179648 | tf_op jit(solution)/shard_map/all_gather | solution.py:28
  135.2 82.5 %all-gather.5.cloned.1.call-start = ((), (), s32[]{:S(2)}) async-start(), calls=%async_computation.2 | async-start | bytes 1179648 | tf_op jit(solution)/shard_map/all_gather | solution.py:28
  135.3 6.4 %collective-permute-start = (f32[256,4]{0,1:T(4,128)S(1)}, f32[256,4]{0,1:T(4,128)S(1)}, u32[]{:S(2)}, u32[]{:S(2)}) collective-permute-start(f32[256,4]{0,1:T(4,128)S(1)} %fusion.28), channel_id=1, source_target_pairs={{0,4},{4,8},{8,12},{12,16},{16,20},{20,24},{24,28},{28,0},{1,5},{5... | collective-permute-start | bytes 12296 | tf_op jit(solution)/shard_map/ppermute | solution.py:15
  141.7 6.3 %collective-permute-start.1 = (f32[256,4]{0,1:T(4,128)S(1)}, f32[256,4]{0,1:T(4,128)S(1)}, u32[]{:S(2)}, u32[]{:S(2)}) collective-permute-start(f32[256,4]{0,1:T(4,128)S(1)} %collective-permute-done), channel_id=1, source_target_pairs={{0,4},{4,8},{8,12},{12,16},{16,20},{20,24},{24,28},{28,0},{1,5},{5... | collective-permute-start | bytes 12296 | tf_op jit(solution)/shard_map/ppermute | solution.py:15
  148.0 6.3 %collective-permute-start.2 = (f32[256,4]{0,1:T(4,128)S(1)}, f32[256,4]{0,1:T(4,128)S(1)}, u32[]{:S(2)}, u32[]{:S(2)}) collective-permute-start(f32[256,4]{0,1:T(4,128)S(1)} %collective-permute-done.1), channel_id=1, source_target_pairs={{0,4},{4,8},{8,12},{12,16},{16,20},{20,24},{24,28},{28,0},{1,5},{5... | collective-permute-start | bytes 12296 | tf_op jit(solution)/shard_map/ppermute | solution.py:15
  154.3 6.4 %collective-permute-start.3 = (f32[256,4]{0,1:T(4,128)S(1)}, f32[256,4]{0,1:T(4,128)S(1)}, u32[]{:S(2)}, u32[]{:S(2)}) collective-permute-start(f32[256,4]{0,1:T(4,128)S(1)} %collective-permute-done.2), channel_id=1, source_target_pairs={{0,4},{4,8},{8,12},{12,16},{16,20},{20,24},{24,28},{28,0},{1,5},{5... | collective-permute-start | bytes 12296 | tf_op jit(solution)/shard_map/ppermute | solution.py:15
  154.3 97.7 %reduce-scatter.2.cloned.1.call-start = ((), (), s32[]{:S(2)}) async-start(), calls=%async_computation.3 | async-start | bytes 655360 | tf_op jit(solution)/shard_map/reduce_scatter | solution.py:36
  160.7 6.4 %collective-permute-start.4 = (f32[256,4]{0,1:T(4,128)S(1)}, f32[256,4]{0,1:T(4,128)S(1)}, u32[]{:S(2)}, u32[]{:S(2)}) collective-permute-start(f32[256,4]{0,1:T(4,128)S(1)} %collective-permute-done.3), channel_id=1, source_target_pairs={{0,4},{4,8},{8,12},{12,16},{16,20},{20,24},{24,28},{28,0},{1,5},{5... | collective-permute-start | bytes 12296 | tf_op jit(solution)/shard_map/ppermute | solution.py:15
  167.1 6.4 %collective-permute-start.5 = (f32[256,4]{0,1:T(4,128)S(1)}, f32[256,4]{0,1:T(4,128)S(1)}, u32[]{:S(2)}, u32[]{:S(2)}) collective-permute-start(f32[256,4]{0,1:T(4,128)S(1)} %collective-permute-done.4), channel_id=1, source_target_pairs={{0,4},{4,8},{8,12},{12,16},{16,20},{20,24},{24,28},{28,0},{1,5},{5... | collective-permute-start | bytes 12296 | tf_op jit(solution)/shard_map/ppermute | solution.py:15
  173.5 31.8 %collective-permute-start.6 = (f32[256,4]{0,1:T(4,128)S(1)}, f32[256,4]{0,1:T(4,128)S(1)}, u32[]{:S(2)}, u32[]{:S(2)}) collective-permute-start(f32[256,4]{0,1:T(4,128)S(1)} %collective-permute-done.5), channel_id=1, source_target_pairs={{0,4},{4,8},{8,12},{12,16},{16,20},{20,24},{24,28},{28,0},{1,5},{5... | collective-permute-start | bytes 12296 | tf_op jit(solution)/shard_map/ppermute | solution.py:15
  211.2 3.2 %copy-start = (f32[4,256,2048]{2,1,0:T(8,128)}, f32[4,256,2048]{2,1,0:T(8,128)S(1)}, u32[]{:S(2)}) copy-start(f32[4,256,2048]{2,1,0:T(8,128)S(1)} %get-tuple-element.13) | copy-start | bytes 25165828
  217.7 35.4 %copy-start.3 = (f32[1024]{0:T(1024)S(1)}, f32[1024]{0:T(1024)}, u32[]{:S(2)}) copy-start(f32[1024]{0:T(1024)} %param.17) | copy-start | bytes 12292
Sparse Core Ops, SparseCore 0:
  135.3 37.2 all-gather.2
  174.6 38.7 all-gather.4
  229.4 22.5 reduce-scatter.1
